TPU v7x, 32 devices: a whole 2x2x4 slice. The times are simulated.
32 devices in a mesh: sp: 16 (over z, y, x), tp: 2 (over core).
Axes of the slice: x: 2, y: 2, z: 4, core: 2. Of those that a mesh axis runs over, the one named last changes fastest.
Arguments:
- tokens: bfloat16 [3072, 4096], P('sp'), may hold values from -6 to 6
- norm_gain: float32 [4096], replicated, may hold values from 0.1 to 1.9
- conv_value: bfloat16 [4096, 2048], P('sp', 'tp'), may hold values from -0.09375 to 0.09375
- conv_gate: bfloat16 [4096, 2048], P('sp', 'tp'), may hold values from -0.09375 to 0.09375
- state_feed: bfloat16 [4096, 2048], P('sp', 'tp'), may hold values from -0.09375 to 0.09375
- conv_taps: float32 [31, 2048], P(None, 'tp'), may hold values from -1 to 1
- chan_gain: float32 [2048], replicated, may hold values from 0.1 to 1.9
- chan_shift: float32 [2048], replicated, may hold values from -3 to 3
- conv_project: bfloat16 [2048, 4096], P('sp', 'tp'), may hold values from -0.125 to 0.125
- decay_rate: float32 [128, 64], P('tp'), may hold values from 0.1 to 3
- frequency: float32 [128, 64], P('tp'), may hold values from 0.1 to 3
- input_real: float32 [128, 64, 16], P('tp'), may hold values from -0.0390625 to 0.0390625
- input_imag: float32 [128, 64, 16], P('tp'), may hold values from -0.0390625 to 0.0390625
- output_real: float32 [128, 16, 64], P('tp'), may hold values from -0.5 to 0.5
- output_imag: float32 [128, 16, 64], P('tp'), may hold values from -0.5 to 0.5
- skip_gain: float32 [2048], P('tp'), may hold values from -3 to 3
- state_value: bfloat16 [2048, 4096], P('sp', 'tp'), may hold values from -0.125 to 0.125
- state_gate: bfloat16 [2048, 4096], P('sp', 'tp'), may hold values from -0.125 to 0.125
- initial_state: float32 [2, 128, 64], P(None, 'tp'), may hold values from -5 to 5
Outputs:
- mixer_out: bfloat16 [3072, 4096], P('sp', 'tp')
- final_state: float32 [2, 128, 64], P(None, 'tp')
All inputs are finite; a program needn't handle non-finite values.
Results may differ from a plain program's by a relative error of at most 0.0085.
Values may be sent and summed in bfloat16 or wider, within the bound.
A program may use at most 128 MiB of HBM per device.

v0:
```python
import functools
import jax
import jax.numpy as jnp
from jax import lax
from jax.experimental import pallas as pl
from jax.experimental.pallas import tpu as pltpu
from jax.sharding import PartitionSpec as P


def passed_along(value, axis, steps):
    count = lax.axis_size(axis)
    leading, last = (max(0, -steps), min(count, count - steps))
    return lax.ppermute(value, axis, [(source, source + steps) for source in range(leading, last)])


def rotate(first_real, first_imag, second_real, second_imag):
    return (
        first_real * second_real - first_imag * second_imag,
        first_real * second_imag + first_imag * second_real,
    )


def power_table(base_real, base_imag, exponent, largest):
    result_real = jnp.ones((exponent.shape[0], base_real.shape[0]), jnp.float32)
    result_imag = jnp.zeros((exponent.shape[0], base_real.shape[0]), jnp.float32)
    square_real, square_imag = (base_real, base_imag)
    for place in range(max(largest, 1).bit_length()):
        chosen = (exponent >> place & 1 == 1)[:, None]
        next_real, next_imag = rotate(result_real, result_imag, square_real, square_imag)
        result_real = jnp.where(chosen, next_real, result_real)
        result_imag = jnp.where(chosen, next_imag, result_imag)
        square_real, square_imag = rotate(square_real, square_imag, square_real, square_imag)
    return (result_real, result_imag)


def local(
    tokens,
    norm_gain,
    conv_value,
    conv_gate,
    state_feed,
    conv_taps,
    chan_gain,
    chan_shift,
    conv_project,
    decay_rate,
    frequency,
    input_real,
    input_imag,
    output_real,
    output_imag,
    skip_gain,
    state_value,
    state_gate,
    initial_state,
):
    highest = lax.Precision.HIGHEST
    floats = tokens.astype(jnp.float32)
    normed = (
        floats * lax.rsqrt(jnp.mean(floats * floats, axis=1, keepdims=True) + 1e-06) * norm_gain
    ).astype(jnp.bfloat16)
    length = tokens.shape[0]
    width = conv_value.shape[1]
    in_block = jnp.concatenate([conv_value, conv_gate, state_feed], axis=1)
    projected = jnp.dot(
        normed,
        lax.all_gather(in_block, "sp", axis=0, tiled=True),
        preferred_element_type=jnp.float32,
    )
    gated_linear = (projected[:, :width] * jax.nn.sigmoid(projected[:, width : 2 * width])).astype(
        jnp.bfloat16
    )
    state_drive = projected[:, 2 * width :].astype(jnp.bfloat16)
    kernel = conv_taps.shape[0]
    before = passed_along(gated_linear[length - (kernel - 1) :], "sp", 1)
    padded = jnp.concatenate([before, gated_linear], axis=0).astype(jnp.float32)
    conv_sum = jnp.zeros((length, width), jnp.float32)
    for offset in range(kernel):
        conv_sum = conv_sum + conv_taps[offset] * padded[offset : offset + length]
    conv_out = conv_sum.astype(jnp.bfloat16)
    seq_devices = lax.axis_size("sp")
    total_tokens = length * seq_devices
    groups, state_size, group_size = input_real.shape
    flat = groups * state_size
    rate_real = -decay_rate / total_tokens
    magnitude = jnp.exp(rate_real)
    step_real = magnitude * jnp.cos(frequency)
    step_imag = magnitude * jnp.sin(frequency)
    modulus = rate_real * rate_real + frequency * frequency
    lift_real = step_real - 1.0
    factor_real = (lift_real * rate_real + step_imag * frequency) / modulus
    factor_imag = (step_imag * rate_real - lift_real * frequency) / modulus
    drive_real = factor_real[..., None] * input_real - factor_imag[..., None] * input_imag
    drive_imag = factor_real[..., None] * input_imag + factor_imag[..., None] * input_real
    grouped = state_drive.astype(jnp.float32).reshape(length, groups, group_size)
    pushed_real = jnp.einsum("gph,tgh->tgp", drive_real, grouped, precision=highest).reshape(
        length, flat
    )
    pushed_imag = jnp.einsum("gph,tgh->tgp", drive_imag, grouped, precision=highest).reshape(
        length, flat
    )
    base_real = step_real.reshape(flat)
    base_imag = step_imag.reshape(flat)
    square_size = base_real * base_real + base_imag * base_imag
    back_real = base_real / square_size
    back_imag = -base_imag / square_size
    positions = lax.iota(jnp.int32, length)
    counted = positions + 1
    power_real, power_imag = power_table(base_real, base_imag, counted, length)
    undo_real, undo_imag = power_table(back_real, back_imag, counted, length)
    scaled_real, scaled_imag = rotate(undo_real, undo_imag, pushed_real, pushed_imag)
    lower = (positions[:, None] >= positions[None, :]).astype(jnp.float32)
    summed_real = jnp.dot(lower, scaled_real, precision=highest)
    summed_imag = jnp.dot(lower, scaled_imag, precision=highest)
    local_real, local_imag = rotate(power_real, power_imag, summed_real, summed_imag)
    span_real, span_imag = (power_real[-1], power_imag[-1])
    last_real, last_imag = (local_real[-1], local_imag[-1])
    start_real = initial_state[0].reshape(flat)
    start_imag = initial_state[1].reshape(flat)
    finals = lax.all_gather(jnp.stack([last_real, last_imag])[None], "sp", axis=0, tiled=True)
    position = lax.axis_index("sp")
    device_ids = lax.iota(jnp.int32, seq_devices)
    lag = jnp.maximum(position - 1 - device_ids, 0)
    weight_real, weight_imag = power_table(span_real, span_imag, lag, seq_devices)
    before_mask = (device_ids < position).astype(jnp.float32)[:, None]
    moved_real, moved_imag = rotate(weight_real, weight_imag, finals[:, 0], finals[:, 1])
    lead_real, lead_imag = power_table(
        span_real, span_imag, jnp.stack([position, jnp.int32(seq_devices)]), seq_devices
    )
    opening_real, opening_imag = rotate(lead_real[0], lead_imag[0], start_real, start_imag)
    entry_real = opening_real + jnp.sum(moved_real * before_mask, axis=0)
    entry_imag = opening_imag + jnp.sum(moved_imag * before_mask, axis=0)
    tail_real, tail_imag = power_table(
        span_real, span_imag, seq_devices - 1 - device_ids, seq_devices
    )
    carried_real, carried_imag = rotate(tail_real, tail_imag, finals[:, 0], finals[:, 1])
    closing_real, closing_imag = rotate(lead_real[1], lead_imag[1], start_real, start_imag)
    final_real = closing_real + jnp.sum(carried_real, axis=0)
    final_imag = closing_imag + jnp.sum(carried_imag, axis=0)
    final_state = jnp.stack([final_real, final_imag]).reshape(2, groups, state_size)
    state_real = (power_real * entry_real - power_imag * entry_imag + local_real).reshape(
        length, groups, state_size
    )
    state_imag = (power_real * entry_imag + power_imag * entry_real + local_imag).reshape(
        length, groups, state_size
    )
    response = jnp.einsum("ghp,tgp->tgh", output_real, state_real, precision=highest) - jnp.einsum(
        "ghp,tgp->tgh", output_imag, state_imag, precision=highest
    )
    response = response.reshape(length, groups * group_size) + skip_gain * state_drive.astype(
        jnp.float32
    )
    activated = jax.nn.gelu(response).astype(jnp.bfloat16)
    conv_rows, activated_rows = (
        lax.all_gather(conv_out, "tp", axis=1, tiled=True),
        lax.all_gather(activated, "tp", axis=1, tiled=True),
    )
    conv_full = conv_rows.astype(jnp.float32)
    row_mean = jnp.mean(conv_full, axis=1, keepdims=True)
    centred = conv_full - row_mean
    variance = jnp.mean(centred * centred, axis=1, keepdims=True)
    conv_act = jax.nn.silu(centred * lax.rsqrt(variance + 1e-05) * chan_gain + chan_shift).astype(
        jnp.bfloat16
    )
    columns = conv_project.shape[1]
    out_block = jnp.concatenate([conv_project, state_value, state_gate], axis=1)
    piece = lax.all_gather(out_block, "sp", axis=0, tiled=True)
    conv_branch = jnp.dot(conv_act, piece[:, :columns], preferred_element_type=jnp.float32)
    state_both = jnp.dot(activated_rows, piece[:, columns:], preferred_element_type=jnp.float32)
    mixer_out = (
        conv_branch + state_both[:, :columns] * jax.nn.sigmoid(state_both[:, columns:])
    ).astype(jnp.bfloat16)
    return (mixer_out, final_state)


def power_stack(base_real, base_imag, count):
    real, imag = (base_real[None], base_imag[None])
    while real.shape[0] < count:
        next_real, next_imag = rotate(real, imag, real[-1:], imag[-1:])
        real = jnp.concatenate([real, next_real], axis=0)
        imag = jnp.concatenate([imag, next_imag], axis=0)
    return (real[:count], imag[:count])


def block_diagonal(blocks):
    groups = blocks.shape[1]
    return blocks[:, :, :, None, :] * jnp.eye(groups, dtype=blocks.dtype)[None, :, None, :, None]


def chunk_matrices(decay_rate, frequency, input_real, input_imag, output_real, output_imag, total, chunk):
    highest = lax.Precision.HIGHEST
    groups, states, width = input_real.shape
    rate_real = -decay_rate / total
    magnitude = jnp.exp(rate_real)
    step_real = magnitude * jnp.cos(frequency)
    step_imag = magnitude * jnp.sin(frequency)
    modulus = rate_real * rate_real + frequency * frequency
    lift_real = step_real - 1.0
    factor_real = (lift_real * rate_real + step_imag * frequency) / modulus
    factor_imag = (step_imag * rate_real - lift_real * frequency) / modulus
    drive_real = factor_real[..., None] * input_real - factor_imag[..., None] * input_imag
    drive_imag = factor_real[..., None] * input_imag + factor_imag[..., None] * input_real
    power_real, power_imag = power_stack(step_real, step_imag, chunk)
    whole_real = jnp.concatenate([jnp.ones_like(step_real)[None], power_real], axis=0)
    whole_imag = jnp.concatenate([jnp.zeros_like(step_imag)[None], power_imag], axis=0)
    back_real = whole_real[:chunk][::-1, :, :, None]
    back_imag = whole_imag[:chunk][::-1, :, :, None]
    push_real, push_imag = rotate(back_real, back_imag, drive_real[None], drive_imag[None])
    push = [
        block_diagonal(value.transpose(0, 1, 3, 2)).reshape(chunk * groups * width, groups * states)
        for value in (push_real, push_imag)
    ]
    push = jnp.concatenate(push, axis=1)
    out_real, out_imag = rotate(
        output_real[None], output_imag[None], whole_real[:, :, None, :], whole_imag[:, :, None, :]
    )
    emit = [
        block_diagonal(value.transpose(1, 3, 0, 2).reshape(1, groups, states, chunk * width))
        for value in (out_real[1:], -out_imag[1:])
    ]
    emit = [
        value.reshape(groups, states, groups, chunk, width)
        .transpose(0, 1, 3, 2, 4)
        .reshape(groups * states, chunk * groups * width)
        for value in emit
    ]
    emit = jnp.concatenate(emit, axis=0)
    response = jnp.einsum(
        "dghp,gpi->dgih", out_real[:chunk], drive_real, precision=highest
    ) - jnp.einsum("dghp,gpi->dgih", out_imag[:chunk], drive_imag, precision=highest)
    spread = block_diagonal(response).reshape(chunk, groups * width, groups * width)
    spread = spread.transpose(1, 0, 2).reshape(groups * width, chunk * groups * width)
    padded = jnp.concatenate([jnp.zeros_like(spread), spread], axis=1)
    span = groups * width
    full = chunk * span
    inside = jnp.concatenate(
        [padded[:, full - place * span : 2 * full - place * span] for place in range(chunk)], axis=0
    )
    return (power_real[-1].reshape(-1), power_imag[-1].reshape(-1), push, emit, inside)


def recurrence(feed, skip_gain, start, matrices, chunk):
    highest = lax.Precision.HIGHEST
    span_real, span_imag, push, emit, inside = matrices
    length, width = feed.shape
    count = length // chunk
    rows = feed.reshape(count, chunk * width).astype(jnp.float32)
    pushed = jnp.dot(rows, push, precision=highest)
    flat = span_real.shape[0]
    first_real, first_imag = rotate(span_real, span_imag, start[0], start[1])
    head = jnp.concatenate([first_real, first_imag])[None]
    pushed = jnp.concatenate([pushed[:1] + head, pushed[1:]], axis=0)
    real, imag = (pushed[:, :flat], pushed[:, flat:])
    shift = 1
    while shift < count:
        moved_real = jnp.pad(real[:-shift], ((shift, 0), (0, 0)))
        moved_imag = jnp.pad(imag[:-shift], ((shift, 0), (0, 0)))
        add_real, add_imag = rotate(span_real, span_imag, moved_real, moved_imag)
        real, imag = (real + add_real, imag + add_imag)
        span_real, span_imag = rotate(span_real, span_imag, span_real, span_imag)
        shift *= 2
    entry_real = jnp.concatenate([start[0][None], real[:-1]], axis=0)
    entry_imag = jnp.concatenate([start[1][None], imag[:-1]], axis=0)
    entry = jnp.concatenate([entry_real, entry_imag], axis=1)
    response = jnp.dot(rows, inside, precision=highest) + jnp.dot(entry, emit, precision=highest)
    response = response + jnp.tile(skip_gain, chunk) * rows
    activated = jax.nn.gelu(response).astype(jnp.bfloat16).reshape(length, width)
    return (activated, jnp.stack([real[-1], imag[-1]]))


def remote(source, target, send_sem, recv_sem, device):
    return pltpu.make_async_remote_copy(
        src_ref=source,
        dst_ref=target,
        send_sem=send_sem,
        recv_sem=recv_sem,
        device_id=device,
        device_id_type=pl.DeviceIdType.MESH,
    )


def plane_neighbours(inner, core):
    flip_x = inner + 1 - 2 * (inner % 2)
    flip_y = inner + 2 - 4 * (inner // 2)
    first = flip_x * (1 - core) + flip_y * core
    second = flip_y * (1 - core) + flip_x * core
    return (first, second, 3 - inner)


def entry_kernel(
    depth, own_ref, in_ref, out_ref, all_ref, taken_ref, moved_ref, sent, landed, in_sent, in_landed,
    out_sent, out_landed, local_sem
):
    outer, inner, core = (lax.axis_index("outer"), lax.axis_index("inner"), lax.axis_index("tp"))
    first, second, opposite = plane_neighbours(inner, core)
    length = own_ref.shape[0]
    devices = 4 * depth
    here = outer * 4 + inner
    half = devices // 2
    target_core = here // half

    def slot(index):
        return all_ref.at[pl.ds(pl.multiple_of(index * length, length), length)]

    def send(index, lane, device, source=None):
        return remote(
            slot(index) if source is None else source,
            slot(index),
            sent.at[index, lane],
            landed.at[index],
            device,
        )

    def arrived(index):
        send(index, 0, (outer, first, core)).wait_recv()

    def spread(index, source=None):
        send(index, 0, (outer, first, core), source).start()
        send(index, 1, (outer, second, core), source).start()

    up, down = ((outer + 1, inner, core), (outer - 1, inner, core))

    @pl.when(outer < depth - 1)
    def _():
        send(here, 2, up, own_ref).start()

    @pl.when(outer > 0)
    def _():
        send(here, 3, down, own_ref).start()

    spread(here, own_ref)
    keep = pltpu.make_async_copy(own_ref, slot(here), local_sem.at[0])
    keep.start()
    place = core * half + here % half

    def in_copy(offset):
        other = (here + offset) % devices
        return remote(
            in_ref.at[other],
            taken_ref.at[place],
            in_sent.at[offset],
            in_landed.at[place],
            (other // 4, other % 4, target_core),
        )

    in_keep = pltpu.make_async_copy(in_ref.at[here], taken_ref.at[place], local_sem.at[1])

    @pl.when(core == target_core)
    def _():
        in_keep.start()

    @pl.when(core != target_core)
    def _():
        in_copy(0).start()

    for offset in range(1, devices):
        in_copy(offset).start()

    out_keep = pltpu.make_async_copy(out_ref.at[inner], moved_ref.at[inner], local_sem.at[2])
    out_keep.start()

    def out_copy(offset):
        other = (inner + offset) % 4
        return remote(
            out_ref.at[other],
            moved_ref.at[inner],
            out_sent.at[offset - 1],
            out_landed.at[inner],
            (outer, other, core),
        )

    for offset in range(1, 4):
        out_copy(offset).start()

    def side(z):
        index = z * 4 + first
        arrived(index)
        send(index, 1, (outer, second, core)).start()

    side(outer)
    for step in range(1, depth):
        below, above = (outer - step, outer + step)

        @pl.when(below >= 0)
        def _():
            index = below * 4 + inner
            arrived(index)

            @pl.when(outer < depth - 1)
            def _():
                send(index, 2, up).start()

            spread(index)

        @pl.when(above < depth)
        def _():
            index = above * 4 + inner
            arrived(index)

            @pl.when(outer > 0)
            def _():
                send(index, 3, down).start()

            spread(index)

        @pl.when(below >= 0)
        def _():
            side(below)

        @pl.when(above < depth)
        def _():
            side(above)

    for z in range(depth):
        arrived(z * 4 + second)
        arrived(z * 4 + opposite)

    for z in range(depth):
        index = z * 4 + inner
        send(index, 0, (outer, first, core)).wait_send()
        send(index, 1, (outer, second, core)).wait_send()
        send(z * 4 + first, 1, (outer, second, core)).wait_send()

        @pl.when(jnp.logical_and(outer < depth - 1, z <= outer))
        def _():
            send(index, 2, up).wait_send()

        @pl.when(jnp.logical_and(outer > 0, z >= outer))
        def _():
            send(index, 3, down).wait_send()

    keep.wait()

    @pl.when(core == target_core)
    def _():
        in_keep.wait()

    @pl.when(core != target_core)
    def _():
        in_copy(0).wait_send()

    for offset in range(1, devices):
        in_copy(offset).wait_send()

    def in_wait(index):
        remote(
            in_ref.at[0],
            taken_ref.at[index],
            in_sent.at[0],
            in_landed.at[index],
            (outer, first, core),
        ).wait_recv()

    for lane in range(2):
        for index in range(half):
            local_one = jnp.logical_and(here == core * half + index, core == lane)

            @pl.when(jnp.logical_not(local_one))
            def _():
                in_wait(lane * half + index)

    out_keep.wait()
    for offset in range(1, 4):
        out_copy(offset).wait_send()
    for offset in range(1, 4):
        other = (inner + offset) % 4
        remote(
            out_ref.at[0],
            moved_ref.at[other],
            out_sent.at[0],
            out_landed.at[other],
            (outer, first, core),
        ).wait_recv()


def entry_exchange(own_half, in_block, out_block, depth):
    devices = 4 * depth
    length, half = own_half.shape
    any_spec = pl.BlockSpec(memory_space=pl.ANY)
    dma = pltpu.SemaphoreType.DMA
    return pl.pallas_call(
        functools.partial(entry_kernel, depth),
        out_shape=(
            jax.ShapeDtypeStruct((devices * length, half), own_half.dtype),
            jax.ShapeDtypeStruct(in_block.shape, in_block.dtype),
            jax.ShapeDtypeStruct(out_block.shape, out_block.dtype),
        ),
        in_specs=[any_spec] * 3,
        out_specs=(any_spec,) * 3,
        scratch_shapes=[
            dma((devices, 4)),
            dma((devices,)),
            dma((devices,)),
            dma((devices,)),
            dma((3,)),
            dma((4,)),
            dma((3,)),
        ],
        compiler_params=pltpu.CompilerParams(has_side_effects=True),
        cost_estimate=pl.CostEstimate(flops=0, bytes_accessed=0, transcendentals=0),
    )(own_half, in_block, out_block)


def middle_kernel(depth, mixed_ref, last_ref, turned_ref, states_ref, sent, landed, last_sent, last_landed, local_sem):
    outer, inner, core = (lax.axis_index("outer"), lax.axis_index("inner"), lax.axis_index("tp"))
    devices = 4 * depth
    here = outer * 4 + inner
    keep = pltpu.make_async_copy(mixed_ref.at[here], turned_ref.at[here], local_sem.at[0])
    keep_last = pltpu.make_async_copy(last_ref, states_ref.at[here], local_sem.at[1])
    keep.start()
    keep_last.start()

    def copies(offset):
        other = (here + offset) % devices
        device = (other // 4, other % 4, core)
        return (
            remote(
                mixed_ref.at[other], turned_ref.at[here], sent.at[offset], landed.at[here], device
            ),
            remote(
                last_ref, states_ref.at[here], last_sent.at[offset], last_landed.at[here], device
            ),
        )

    for offset in range(1, devices):
        for copy in copies(offset):
            copy.start()
    keep.wait()
    keep_last.wait()
    for offset in range(1, devices):
        for copy in copies(offset):
            copy.wait_send()
    for offset in range(1, devices):
        other = (here + offset) % devices
        device = (other // 4, other % 4, core)
        remote(
            mixed_ref.at[other], turned_ref.at[other], sent.at[offset], landed.at[other], device
        ).wait_recv()
        remote(
            last_ref, states_ref.at[other], last_sent.at[offset], last_landed.at[other], device
        ).wait_recv()


def middle_exchange(mixed, last, depth):
    devices = 4 * depth
    any_spec = pl.BlockSpec(memory_space=pl.ANY)
    dma = pltpu.SemaphoreType.DMA
    return pl.pallas_call(
        functools.partial(middle_kernel, depth),
        out_shape=(
            jax.ShapeDtypeStruct(mixed.shape, mixed.dtype),
            jax.ShapeDtypeStruct((devices,) + last.shape, last.dtype),
        ),
        in_specs=[any_spec] * 2,
        out_specs=(any_spec,) * 2,
        scratch_shapes=[dma((devices,))] * 4 + [dma((2,))],
        compiler_params=pltpu.CompilerParams(has_side_effects=True),
    )(mixed, last)


def channel_local(
    tokens,
    norm_gain,
    conv_value,
    conv_gate,
    state_feed,
    conv_taps,
    chan_gain,
    chan_shift,
    conv_project,
    decay_rate,
    frequency,
    input_real,
    input_imag,
    output_real,
    output_imag,
    skip_gain,
    state_value,
    state_gate,
    initial_state,
):
    seq = ("outer", "inner")
    devices = lax.axis_size("outer") * lax.axis_size("inner")
    inner = lax.axis_size("inner")
    position = lax.axis_index("outer") * inner + lax.axis_index("inner")
    core = lax.axis_index("tp")
    swap = [(0, 1), (1, 0)]
    local_length, model = tokens.shape
    total = local_length * devices
    half = model // 2
    floats = tokens.astype(jnp.float32)
    normed = (
        floats * lax.rsqrt(jnp.mean(floats * floats, axis=1, keepdims=True) + 1e-06) * norm_gain
    ).astype(jnp.bfloat16)
    own_half = lax.dynamic_slice_in_dim(normed, core * half, half, axis=1)
    rows, wide = conv_value.shape
    share = wide // devices
    in_block = jnp.stack([conv_value, conv_gate, state_feed], axis=1)
    in_block = in_block.reshape(rows, 3, devices, share).transpose(2, 0, 1, 3)
    in_block = in_block.reshape(devices, rows, 3 * share)
    out_rows, columns = conv_project.shape
    piece = columns // inner
    out_block = jnp.stack([conv_project, state_value, state_gate], axis=1)
    out_block = out_block.reshape(out_rows, 3, inner, piece).transpose(2, 0, 1, 3)
    out_block = out_block.reshape(inner, out_rows, 3 * piece)
    all_half, in_block, out_block = entry_exchange(
        own_half, in_block, out_block, lax.axis_size("outer")
    )
    in_block = in_block.reshape(2, half, 3 * share)
    kept = lax.dynamic_index_in_dim(in_block, core, axis=0, keepdims=False)
    taken = lax.dynamic_index_in_dim(in_block, 1 - core, axis=0, keepdims=False)
    out_block = lax.all_gather(
        out_block.reshape(inner * out_rows, 3 * piece), "outer", axis=0, tiled=True
    )
    groups = decay_rate.shape[0] // devices
    chunk = 16

    def own(value, axis=0, size=groups):
        return lax.dynamic_slice_in_dim(value, position * size, size, axis=axis)

    matrices = chunk_matrices(
        own(decay_rate),
        own(frequency),
        own(input_real),
        own(input_imag),
        own(output_real),
        own(output_imag),
        total,
        chunk,
    )
    other = lax.ppermute(jnp.dot(all_half, taken, preferred_element_type=jnp.float32), "tp", swap)
    projected = jnp.dot(all_half, kept, preferred_element_type=jnp.float32) + other
    gated = (projected[:, :share] * jax.nn.sigmoid(projected[:, share : 2 * share])).astype(
        jnp.bfloat16
    )
    feed = projected[:, 2 * share :].astype(jnp.bfloat16)
    kernel = conv_taps.shape[0]
    taps = own(conv_taps, 1, share)
    padded = jnp.pad(gated, ((kernel - 1, 0), (0, 0))).astype(jnp.float32)
    conv_sum = jnp.zeros((total, share), jnp.float32)
    for offset in range(kernel):
        conv_sum = conv_sum + taps[offset] * padded[offset : offset + total]
    conv_out = conv_sum.astype(jnp.bfloat16)
    start = own(initial_state, 1).reshape(2, -1)
    activated, last = recurrence(feed, own(skip_gain, 0, share), start, matrices, chunk)
    states = initial_state.shape[2]
    mixed = jnp.concatenate([conv_out, activated], axis=1).reshape(devices, local_length, 2 * share)
    mixed, last = middle_exchange(mixed, last.reshape(-1, 128), lax.axis_size("outer"))
    mixed = mixed.transpose(1, 0, 2)
    final_state = last.reshape(devices, 2, groups, states).transpose(1, 0, 2, 3)
    final_state = final_state.reshape(initial_state.shape)
    conv_full = mixed[:, :, :share].reshape(local_length, wide).astype(jnp.float32)
    active = mixed[:, :, share:].reshape(local_length, wide)
    own_mean = jnp.mean(conv_full, axis=1, keepdims=True)
    deviation = conv_full - own_mean
    own_spread = jnp.mean(deviation * deviation, axis=1, keepdims=True)
    peer = lax.ppermute(jnp.concatenate([own_mean, own_spread], axis=1), "tp", swap)
    row_mean = 0.5 * (own_mean + peer[:, :1])
    gap = 0.5 * (own_mean - peer[:, :1])
    variance = 0.5 * (own_spread + peer[:, 1:]) + gap * gap
    gain = lax.dynamic_slice_in_dim(chan_gain, core * wide, wide, axis=0)
    bias = lax.dynamic_slice_in_dim(chan_shift, core * wide, wide, axis=0)
    conv_act = jax.nn.silu(
        (conv_full - row_mean) * lax.rsqrt(variance + 1e-05) * gain + bias
    ).astype(jnp.bfloat16)
    both = jnp.stack([conv_act, active], axis=0)
    both = lax.all_gather(both, "inner", axis=1, tiled=True)
    both = lax.all_gather(both, "tp", axis=2, tiled=True)
    conv_branch = jnp.dot(both[0], out_block[:, :piece], preferred_element_type=jnp.float32)
    state_both = jnp.dot(both[1], out_block[:, piece:], preferred_element_type=jnp.float32)
    mixer = (conv_branch + state_both[:, :piece] * jax.nn.sigmoid(state_both[:, piece:])).astype(
        jnp.bfloat16
    )
    mixer = mixer.reshape(inner, local_length, piece)
    mixer = lax.all_to_all(mixer, "inner", 0, 0, tiled=True)
    mixer_out = mixer.transpose(1, 0, 2).reshape(local_length, columns)
    return (mixer_out, final_state)


def specs_of(seq):
    in_specs = (
        P(seq, None),
        P(),
        P(seq, "tp"),
        P(seq, "tp"),
        P(seq, "tp"),
        P(None, "tp"),
        P(),
        P(),
        P(seq, "tp"),
        P("tp", None),
        P("tp", None),
        P("tp", None, None),
        P("tp", None, None),
        P("tp", None, None),
        P("tp", None, None),
        P("tp"),
        P(seq, "tp"),
        P(seq, "tp"),
        P(None, "tp", None),
    )
    return (in_specs, (P(seq, "tp"), P(None, "tp", None)))


def solution(mesh):
    seq_devices, cores = (mesh.shape["sp"], mesh.shape["tp"])
    fine = jax.sharding.Mesh(
        mesh.devices.reshape(seq_devices // 4, 4, cores), ("outer", "inner", "tp")
    )

    def run(*args):
        groups = args[9].shape[0]
        if cores == 2 and groups % (cores * seq_devices) == 0:
            in_specs, out_specs = specs_of(("outer", "inner"))
            body = jax.shard_map(
                channel_local, mesh=fine, in_specs=in_specs, out_specs=out_specs, check_vma=False
            )
        else:
            in_specs, out_specs = specs_of("sp")
            body = jax.shard_map(
                local, mesh=mesh, in_specs=in_specs, out_specs=out_specs, check_vma=False
            )
        return body(*args)

    return run
```

profile of v0, /device:TPU:0, one launch (start us, length us, event | category | flops | bytes accessed | tf_op | source)
XLA Modules:
  0.0 527.2 jit_solution(327121091383144665)
XLA Ops:
  18.5 3.7 copy.87.in_ref
  28.4 2.7 pad_maximum_fusion
  31.0 2.7 copy.88.out_ref
  34.8 152.1 %shard_map.194 = (bf16[3072,2048]{1,0:T(8,128)(2,1)}, bf16[16,256,192]{2,1,0:T(8,128)(2,1)}, bf16[4,128,1536]{2,1,0:T(8,128)(2,1)}) custom-call(bf16[192,2048]{1,0:T(8,128)(2,1)} %fusion.18.own_ref, bf16[16,256,192]{2,1,0:T(8,128)(2,1)} %copy.87.in_ref, bf16[4,128,1536]{2,1,0:T(8,128)(2,1)} %copy.88.out_ref), custom_call_target="tpu_custom_call" | custom-call | tf_op jit(solution)/shard_map/pallas_call | solution.py:481
  186.9 10.5 %fusion.27 = f32[3072,192]{0,1:T(8,128)} fusion(bf16[3072,2048]{1,0:T(8,128)(2,1)} %get-tuple-element.7, bf16[2,2048,192]{2,1,0:T(8,128)(2,1)} %bitcast.191, s32[]{:T(128)S(6)} %select_n.30), kind=kOutput, calls=%fused_computation.54 | convolution fusion | flops 2415919104 | bytes 15990788 | tf_op jit(solution)/shard_map/dot_general | solution.py:631
  197.4 4.6 collective-permute-start
  205.4 4.5 fusion.79
  210.8 4.5 fusion.23
  220.3 3.2 broadcast_multiply_fusion.3
  223.6 2.6 broadcast_multiply_fusion.1
  226.5 3.2 mul.1748
  229.8 3.2 mul.1753
  244.8 9.6 %convolution_add_fusion = f32[3072,192]{0,1:T(8,128)S(1)} fusion(f32[3072,192]{0,1:T(8,128)} %collective-permute-done, bf16[3072,2048]{1,0:T(8,128)(2,1)} %get-tuple-element.7, bf16[2,2048,192]{2,1,0:T(8,128)(2,1)S(1)} %bitcast.192, s32[]{:T(128)S(6)} %select_n.29), kind=kOutput, calls=%fused_computation.2 | convolution fusion | flops 2416508928 | bytes 18350084 | tf_op jit(solution)/shard_map/dot_general | solution.py:632
  258.3 2.8 reshape.484
  270.4 7.3 %fusion.41 = bf16[3072,64]{0,1:T(8,128)(2,1)S(1)} fusion(f32[3102,64]{0,1:T(8,128)S(1)} %pad_convert_fusion, f32[64]{0:T(128)S(1)} %copy-done.25, f32[64]{0:T(128)S(1)} %get-tuple-element.65, f32[64]{0:T(128)S(1)} %get-tuple-element.66, f32[64]{0:T(128)S(1)} %get-tuple-element.67, f32[64]{0:T(128)S(1)} %get-tuple-element.68, f32[64]{0:T(128)S(1)} %get-tuple-element.69, ...), kind=kLoop, calls=%fused_computation.76 | loop fusion | flops 12189696 | bytes 24780544 | tf_op jit(solution)/shard_map/convert_element_type | solution.py:643
  280.0 23.0 %shard_map.195 = (bf16[16,192,128]{2,1,0:T(8,128)(2,1)}, f32[16,4,128]{2,1,0:T(4,128)}) custom-call(bf16[16,192,128]{2,1,0:T(8,128)(2,1)} %pad_maximum_fusion.2.mixed_ref, f32[4,128]{1,0:T(4,128)} %reshape.486.last_ref), custom_call_target="tpu_custom_call" | custom-call | tf_op jit(solution)/shard_map/pallas_call | solution.py:548
  312.3 47.8 %all-gather.4.cloned.1.call-done = bf16[2,768,1024]{2,0,1:T(2,128)(2,1)} async-done(((bf16[2,192,1024]{2,0,1:T(2,128)(2,1)}), bf16[2,768,1024]{2,0,1:T(2,128)(2,1)}) %all-gather.4.cloned.1.call-update) | async-done | bytes 3145744 | tf_op jit(solution)/shard_map/all_gather | solution.py:667
  360.1 4.5 copy.101
  364.6 112.4 %all-gather.8.cloned.1.call-done = bf16[2048,1536]{1,0:T(8,128)(2,1)} async-done(((bf16[512,1536]{1,0:T(8,128)(2,1)}), bf16[2048,1536]{1,0:T(8,128)(2,1)}) %all-gather.8.cloned.1.call-update) | async-done | bytes 6291472 | tf_op jit(solution)/shard_map/all_gather | solution.py:612
  477.1 16.5 %all-gather.6.cloned.1.call-done = bf16[2,768,2048]{2,1,0:T(8,128)(2,1)} async-done(((bf16[2,768,1024]{2,1,0:T(8,128)(2,1)}), bf16[2,768,2048]{2,1,0:T(8,128)(2,1)}) %all-gather.6.cloned.1.call-update) | async-done | bytes 6291472 | tf_op jit(solution)/shard_map/all_gather | solution.py:668
  493.6 6.3 %fusion = f32[768,1024]{1,0:T(8,128)S(1)} fusion(bf16[2048,1536]{1,0:T(8,128)(2,1)} %all-gather.8.cloned.1.call-done, bf16[2,768,2048]{2,1,0:T(8,128)(2,1)} %all-gather.6.cloned.1.call-done), kind=kOutput, calls=%fused_computation | convolution fusion | flops 3221225472 | bytes 10485760 | tf_op jit(solution)/shard_map/dot_general | solution.py:670
  499.9 4.4 fusion.19
  504.3 3.9 all-to-all-start
  509.0 10.5 %all-to-all-done = bf16[4,192,512]{2,1,0:T(8,128)(2,1)S(1)} async-done(((bf16[4,192,512]{2,1,0:T(8,128)(2,1)}), bf16[4,192,512]{2,1,0:T(8,128)(2,1)S(1)}, u32[]{:S(2)}, u32[]{:S(2)}) %all-to-all-start) | async-done | bytes 786464 | tf_op jit(solution)/shard_map/all_to_all | solution.py:675
  (203 shorter events, 65.5 us)
Async XLA Ops:
  7.2 353.0 %all-gather.4.cloned.1.call-start = ((), (), s32[]{:S(2)}) async-start(), calls=%async_computation.1 | async-start | bytes 3932160 | tf_op jit(solution)/shard_map/all_gather | solution.py:667
  28.4 5.3 %copy-start.10 = (f32[4096]{0:T(1024)S(1)}, f32[4096]{0:T(1024)}, u32[]{:S(2)}) copy-start(f32[4096]{0:T(1024)} %param.20) | copy-start | bytes 49156
  197.4 47.4 %collective-permute-start = (f32[3072,192]{0,1:T(8,128)}, f32[3072,192]{0,1:T(8,128)}, u32[]{:S(2)}, u32[]{:S(2)}) collective-permute-start(f32[3072,192]{0,1:T(8,128)} %fusion.27), channel_id=1, source_target_pairs={{0,1},{1,0},{2,3},{3,2},{4,5},{5,4},{6,7},{7,6},{8,9},{9,8},{10,11... | collective-permute-start | bytes 7077896 | tf_op jit(solution)/shard_map/ppermute | solution.py:631
  254.4 6.7 %copy-start.4 = (f32[1024,256]{1,0:T(8,128)S(1)}, f32[1024,256]{1,0:T(8,128)}, u32[]{:S(2)}) copy-start(f32[1024,256]{1,0:T(8,128)} %mul.1748) | copy-start | bytes 3145732
  254.4 6.7 %copy-start.5 = (f32[1024,256]{1,0:T(8,128)S(1)}, f32[1024,256]{1,0:T(8,128)}, u32[]{:S(2)}) copy-start(f32[1024,256]{1,0:T(8,128)} %mul.1753) | copy-start | bytes 3145732
  263.9 3.2 copy-start.2
  263.9 3.2 copy-start.6
  267.2 3.0 copy-start.11
  267.2 3.0 copy-start.12
  267.2 3.0 copy-start.13
  267.2 3.0 copy-start.14
  267.2 3.0 copy-start.15
  267.2 3.0 copy-start.16
  267.2 3.0 copy-start.17
  267.2 3.0 copy-start.18
  267.3 3.0 copy-start.19
  267.3 3.0 copy-start.20
  267.3 3.0 copy-start.21
  306.0 2.8 collective-permute-start.1
  311.5 165.5 %all-gather.8.cloned.1.call-start = ((), (), s32[]{:S(2)}) async-start(), calls=%async_computation.3 | async-start | bytes 7864320 | tf_op jit(solution)/shard_map/all_gather | solution.py:612
  312.3 181.3 %all-gather.6.cloned.1.call-start = ((), (), s32[]{:S(2)}) async-start(), calls=%async_computation.2 | async-start | bytes 9437184 | tf_op jit(solution)/shard_map/all_gather | solution.py:668
  493.6 6.3 %copy-start.26 = (bf16[2,768,2048]{2,1,0:T(8,128)(2,1)S(1)}, bf16[2,768,2048]{2,1,0:T(8,128)(2,1)}, u32[]{:S(2)}) copy-start(bf16[2,768,2048]{2,1,0:T(8,128)(2,1)} %all-gather.6.cloned.1.call-done) | copy-start | bytes 18874372
  499.9 8.3 %copy-start.9 = (f32[16,4,128]{2,1,0:T(4,128)S(1)}, f32[16,4,128]{2,1,0:T(4,128)}, u32[]{:S(2)}) copy-start(f32[16,4,128]{2,1,0:T(4,128)} %get-tuple-element.11) | copy-start | bytes 98308
  504.3 15.2 %all-to-all-start = ((bf16[4,192,512]{2,1,0:T(8,128)(2,1)}), bf16[4,192,512]{2,1,0:T(8,128)(2,1)S(1)}, u32[]{:S(2)}, u32[]{:S(2)}) async-start(bf16[4,192,512]{2,1,0:T(8,128)(2,1)} %bitcast.74), calls=%async_computation | async-start | bytes 1572864 | tf_op jit(solution)/shard_map/all_to_all | solution.py:675
  (11 other events, 28.4 us)
Sparse Core Ops, SparseCore 0:
  311.7 48.4 all-gather.3
  361.7 115.3 all-gather.7
  478.6 14.9 all-gather.5
where the time goes:
time: 532 us; the launch traced here: 527 us
  waiting for transfers between devices  188 us (35%)
  Pallas kernels  175 us (33%)
  local copies, waits for them, and re-layouts  61.4 us (12%)
  matrix products  46.3 us (9%)
  other arithmetic  32.7 us (6%)
  between operations  15 us (3%)
  starting transfers between devices  8.66 us (2%)
    pallas_call x1, Pallas kernels, entry_exchange(): pl.pallas_call(functools.partial(entry_kernel, depth), out_shape=(jax.Sha...  152 us
    all_gather x1, waiting for transfers between devices, channel_local(): lax.all_gather(out_block.reshape(inner * out_rows, 3 * piece), 'outer', a...  112 us
    all_gather x1, waiting for transfers between devices, channel_local(): both = lax.all_gather(both, 'inner', axis=1, tiled=True)  47.8 us
    pallas_call x1, Pallas kernels, middle_exchange(): pl.pallas_call(functools.partial(middle_kernel, depth), out_shape=(jax.Sh...  23 us
    all_gather x1, waiting for transfers between devices, channel_local(): both = lax.all_gather(both, 'tp', axis=2, tiled=True)  16.5 us
    unnamed x78, local copies, waits for them, and re-layouts  16 us
    mul x8, local copies, waits for them, and re-layouts, block_diagonal(): blocks[:, :, :, None, :]  12.7 us
  transfers between devices with their start and end apart: 6, of which 4 were waited for; matrix products, arithmetic and copies ran while one was open for 9% of the time, Pallas kernels for 0%

commit v1 on v0

--- a/solution.py
+++ b/solution.py
@@ -288,8 +288,8 @@
 
 
 def entry_kernel(
-    depth, own_ref, in_ref, out_ref, all_ref, taken_ref, moved_ref, sent, landed, in_sent, in_landed,
-    out_sent, out_landed, local_sem
+    depth, own_ref, in_ref, project_ref, value_ref, gate_ref, all_ref, taken_ref, moved_ref, sent,
+    landed, in_sent, in_landed, out_sent, out_landed, local_sem
 ):
     outer, inner, core = (lax.axis_index("outer"), lax.axis_index("inner"), lax.axis_index("tp"))
     first, second, opposite = plane_neighbours(inner, core)
@@ -356,21 +356,36 @@
     for offset in range(1, devices):
         in_copy(offset).start()
 
-    out_keep = pltpu.make_async_copy(out_ref.at[inner], moved_ref.at[inner], local_sem.at[2])
-    out_keep.start()
-
-    def out_copy(offset):
+    out_refs = (project_ref, value_ref, gate_ref)
+    out_rows, columns = project_ref.shape
+    piece = columns // 4
+
+    def out_from(which, other):
+        return out_refs[which].at[:, pl.ds(pl.multiple_of(other * piece, piece), piece)]
+
+    def out_to(which, origin):
+        rows = pl.ds(pl.multiple_of(origin * out_rows, out_rows), out_rows)
+        return moved_ref.at[rows, pl.ds(which * piece, piece)]
+
+    def out_keep(which):
+        return pltpu.make_async_copy(
+            out_from(which, inner), out_to(which, inner), local_sem.at[2 + which]
+        )
+
+    def out_copy(which, offset):
         other = (inner + offset) % 4
         return remote(
-            out_ref.at[other],
-            moved_ref.at[inner],
-            out_sent.at[offset - 1],
-            out_landed.at[inner],
+            out_from(which, other),
+            out_to(which, inner),
+            out_sent.at[which, offset],
+            out_landed.at[which, inner],
             (outer, other, core),
         )
 
-    for offset in range(1, 4):
-        out_copy(offset).start()
+    for which in range(3):
+        out_keep(which).start()
+        for offset in range(1, 4):
+            out_copy(which, offset).start()
 
     def side(z):
         index = z * 4 + first
@@ -459,23 +474,25 @@
             def _():
                 in_wait(lane * half + index)
 
-    out_keep.wait()
-    for offset in range(1, 4):
-        out_copy(offset).wait_send()
-    for offset in range(1, 4):
-        other = (inner + offset) % 4
-        remote(
-            out_ref.at[0],
-            moved_ref.at[other],
-            out_sent.at[0],
-            out_landed.at[other],
-            (outer, first, core),
-        ).wait_recv()
-
-
-def entry_exchange(own_half, in_block, out_block, depth):
+    for which in range(3):
+        out_keep(which).wait()
+        for offset in range(1, 4):
+            out_copy(which, offset).wait_send()
+        for offset in range(1, 4):
+            other = (inner + offset) % 4
+            remote(
+                out_from(which, other),
+                out_to(which, other),
+                out_sent.at[which, 0],
+                out_landed.at[which, other],
+                (outer, first, core),
+            ).wait_recv()
+
+
+def entry_exchange(own_half, in_block, out_weights, depth):
     devices = 4 * depth
     length, half = own_half.shape
+    out_rows, columns = out_weights[0].shape
     any_spec = pl.BlockSpec(memory_space=pl.ANY)
     dma = pltpu.SemaphoreType.DMA
     return pl.pallas_call(
@@ -483,22 +500,22 @@
         out_shape=(
             jax.ShapeDtypeStruct((devices * length, half), own_half.dtype),
             jax.ShapeDtypeStruct(in_block.shape, in_block.dtype),
-            jax.ShapeDtypeStruct(out_block.shape, out_block.dtype),
+            jax.ShapeDtypeStruct((4 * out_rows, 3 * (columns // 4)), in_block.dtype),
         ),
-        in_specs=[any_spec] * 3,
+        in_specs=[any_spec] * 5,
         out_specs=(any_spec,) * 3,
         scratch_shapes=[
             dma((devices, 4)),
             dma((devices,)),
             dma((devices,)),
             dma((devices,)),
-            dma((3,)),
-            dma((4,)),
-            dma((3,)),
+            dma((3, 4)),
+            dma((3, 4)),
+            dma((5,)),
         ],
         compiler_params=pltpu.CompilerParams(has_side_effects=True),
         cost_estimate=pl.CostEstimate(flops=0, bytes_accessed=0, transcendentals=0),
-    )(own_half, in_block, out_block)
+    )(own_half, in_block, *out_weights)
 
 
 def middle_kernel(depth, mixed_ref, last_ref, turned_ref, states_ref, sent, landed, last_sent, last_landed, local_sem):
@@ -556,6 +573,67 @@
         scratch_shapes=[dma((devices,))] * 4 + [dma((2,))],
         compiler_params=pltpu.CompilerParams(has_side_effects=True),
     )(mixed, last)
+
+
+def exit_kernel(own_ref, all_ref, sent, landed, local_sem):
+    outer, inner, core = (lax.axis_index("outer"), lax.axis_index("inner"), lax.axis_index("tp"))
+    first, second, opposite = plane_neighbours(inner, core)
+    length, half = own_ref.shape[1:]
+
+    def slot(index, side):
+        rows = pl.ds(pl.multiple_of(index * length, length), length)
+        return all_ref.at[:, rows, pl.ds(pl.multiple_of(side * half, half), half)]
+
+    def send(index, lane, device, source=None):
+        return remote(
+            slot(index, core) if source is None else source,
+            slot(index, core),
+            sent.at[index, lane],
+            landed.at[core, index],
+            device,
+        )
+
+    peer = (outer, inner, 1 - core)
+    near, far = ((outer, first, core), (outer, second, core))
+    send(inner, 0, near, own_ref).start()
+    send(inner, 1, far, own_ref).start()
+    send(inner, 2, peer, own_ref).start()
+    keep = pltpu.make_async_copy(own_ref, slot(inner, core), local_sem.at[0])
+    keep.start()
+    send(first, 0, near).wait_recv()
+    send(first, 1, far).start()
+    send(first, 2, peer).start()
+    for index in (second, opposite):
+        send(index, 0, near).wait_recv()
+        send(index, 2, peer).start()
+    for index in range(4):
+        remote(
+            own_ref,
+            slot(index, 1 - core),
+            sent.at[index, 2],
+            landed.at[1 - core, index],
+            peer,
+        ).wait_recv()
+    send(inner, 0, near).wait_send()
+    send(inner, 1, far).wait_send()
+    send(first, 1, far).wait_send()
+    for index in (inner, first, second, opposite):
+        send(index, 2, peer).wait_send()
+    keep.wait()
+
+
+def exit_gather(both):
+    parts, length, half = both.shape
+    any_spec = pl.BlockSpec(memory_space=pl.ANY)
+    dma = pltpu.SemaphoreType.DMA
+    return pl.pallas_call(
+        exit_kernel,
+        out_shape=jax.ShapeDtypeStruct((parts, 4 * length, 2 * half), both.dtype),
+        in_specs=[any_spec],
+        out_specs=any_spec,
+        scratch_shapes=[dma((4, 3)), dma((2, 4)), dma((1,))],
+        compiler_params=pltpu.CompilerParams(has_side_effects=True),
+    )(both)
 
 
 def channel_local(
@@ -600,20 +678,15 @@
     in_block = in_block.reshape(devices, rows, 3 * share)
     out_rows, columns = conv_project.shape
     piece = columns // inner
-    out_block = jnp.stack([conv_project, state_value, state_gate], axis=1)
-    out_block = out_block.reshape(out_rows, 3, inner, piece).transpose(2, 0, 1, 3)
-    out_block = out_block.reshape(inner, out_rows, 3 * piece)
     all_half, in_block, out_block = entry_exchange(
-        own_half, in_block, out_block, lax.axis_size("outer")
+        own_half, in_block, (conv_project, state_value, state_gate), lax.axis_size("outer")
     )
     in_block = in_block.reshape(2, half, 3 * share)
     kept = lax.dynamic_index_in_dim(in_block, core, axis=0, keepdims=False)
     taken = lax.dynamic_index_in_dim(in_block, 1 - core, axis=0, keepdims=False)
-    out_block = lax.all_gather(
-        out_block.reshape(inner * out_rows, 3 * piece), "outer", axis=0, tiled=True
-    )
+    out_block = lax.all_gather(out_block, "outer", axis=0, tiled=True)
     groups = decay_rate.shape[0] // devices
-    chunk = 16
+    chunk = 8
 
     def own(value, axis=0, size=groups):
         return lax.dynamic_slice_in_dim(value, position * size, size, axis=axis)
@@ -664,8 +737,7 @@
         (conv_full - row_mean) * lax.rsqrt(variance + 1e-05) * gain + bias
     ).astype(jnp.bfloat16)
     both = jnp.stack([conv_act, active], axis=0)
-    both = lax.all_gather(both, "inner", axis=1, tiled=True)
-    both = lax.all_gather(both, "tp", axis=2, tiled=True)
+    both = exit_gather(both)
     conv_branch = jnp.dot(both[0], out_block[:, :piece], preferred_element_type=jnp.float32)
     state_both = jnp.dot(both[1], out_block[:, piece:], preferred_element_type=jnp.float32)
     mixer = (conv_branch + state_both[:, :piece] * jax.nn.sigmoid(state_both[:, piece:])).astype(

time: 532 us -> 386 us (0.73)
  waiting for transfers between devices: 188 us -> 10.9 us
  Pallas kernels: 175 us -> 243 us
  local copies, waits for them, and re-layouts: 61.4 us -> 40.9 us
  other arithmetic: 32.7 us -> 26.5 us
    all_gather x3 -> x1, waiting for transfers between devices: 177 us -> 0.02 us  [channel_local(): out_block = lax.all_gather(out_block, 'outer', axis=0, tiled=True)]
    pallas_call x0 -> x1, Pallas kernels: none -> 54 us  [exit_gather(): pl.pallas_call(exit_kernel, out_shape=jax.ShapeDtypeStruct((parts, 4 * le...]
    pallas_call x1, Pallas kernels: 23 us -> 36.5 us  [middle_exchange(): pl.pallas_call(functools.partial(middle_kernel, depth), out_shape=(jax.Sh...]
    unnamed x78 -> x147, local copies, waits for them, and re-layouts: 16 us -> 10.9 us
  transfers between devices with their start and end apart: 6 -> 4, of which waited for: 4 -> 1; matrix products, arithmetic and copies ran while one was open for 9% -> 18% of each run, Pallas kernels for 0% -> 24%
where the time goes in v1:
time: 386 us; the launch traced here: 385 us
  Pallas kernels  243 us (63%)
  matrix products  43.5 us (11%)
  local copies, waits for them, and re-layouts  40.9 us (11%)
  other arithmetic  26.5 us (7%)
  between operations  15.5 us (4%)
  waiting for transfers between devices  10.9 us (3%)
  starting transfers between devices  4.8 us (1%)
    pallas_call x1, Pallas kernels, entry_exchange(): pl.pallas_call(functools.partial(entry_kernel, depth), out_shape=(jax.Sha...  152 us
    pallas_call x1, Pallas kernels, exit_gather(): pl.pallas_call(exit_kernel, out_shape=jax.ShapeDtypeStruct((parts, 4 * le...  54 us
    pallas_call x1, Pallas kernels, middle_exchange(): pl.pallas_call(functools.partial(middle_kernel, depth), out_shape=(jax.Sh...  36.5 us
    unnamed x147, local copies, waits for them, and re-layouts  10.9 us
    all_to_all x1, waiting for transfers between devices, channel_local(): mixer = lax.all_to_all(mixer, 'inner', 0, 0, tiled=True)  10.9 us
    dot_general x1, matrix products, channel_local(): jnp.dot(all_half, taken, preferred_element_type=jnp.float32)  10.5 us
    dot_general x1, matrix products, channel_local(): jnp.dot(all_half, kept, preferred_element_type=jnp.float32) + other  10.1 us
    mul x8, local copies, waits for them, and re-layouts, block_diagonal(): blocks[:, :, :, None, :]  7.85 us
  transfers between devices with their start and end apart: 4, of which 1 were waited for; matrix products, arithmetic and copies ran while one was open for 18% of the time, Pallas kernels for 24%

profile of v1, /device:TPU:0, one launch (start us, length us, event | category | flops | bytes accessed | tf_op | source)
XLA Modules:
  0.0 384.8 jit_solution(18378322718701550922)
XLA Ops:
  7.2 1.9 convert_element_type.98
  9.5 2.0 copy.34
  11.6 2.0 copy.35
  13.6 2.0 copy.36
  18.4 3.7 copy.38.in_ref
  23.2 152.1 %shard_map.194 = (bf16[3072,2048]{1,0:T(8,128)(2,1)}, bf16[16,256,192]{2,1,0:T(8,128)(2,1)}, bf16[512,1536]{1,0:T(8,128)(2,1)}) custom-call(bf16[192,2048]{1,0:T(8,128)(2,1)} %fusion.14.own_ref, bf16[16,256,192]{2,1,0:T(8,128)(2,1)} %copy.38.in_ref, bf16[128,2048]{1,0:T(8,128)(2,1)} %project_ref.1, bf16[128,2048]{1,0:T(8,128)(2,1)} %value_ref.1, ...), custom_call_target="tpu_custom_call" | custom-call | tf_op jit(solution)/shard_map/pallas_call | solution.py:498
  175.3 10.5 %fusion.29 = f32[3072,192]{0,1:T(8,128)} fusion(bf16[3072,2048]{1,0:T(8,128)(2,1)} %get-tuple-element.7, bf16[2,2048,192]{2,1,0:T(8,128)(2,1)} %bitcast.165, s32[]{:T(128)S(6)} %select_n.30), kind=kOutput, calls=%fused_computation.37 | convolution fusion | flops 2415919104 | bytes 15990788 | tf_op jit(solution)/shard_map/dot_general | solution.py:704
  191.8 2.7 fusion.109
  194.5 2.7 fusion.21
  198.6 1.8 fusion.132
  200.4 1.7 dynamic-slice_bitcast_fusion.29
  208.0 2.6 mul.1884
  219.0 10.1 %convolution_add_fusion = f32[3072,192]{0,1:T(8,128)S(1)} fusion(f32[3072,192]{0,1:T(8,128)} %collective-permute-done, bf16[3072,2048]{1,0:T(8,128)(2,1)} %get-tuple-element.7, bf16[2,2048,192]{2,1,0:T(8,128)(2,1)} %bitcast.166, s32[]{:T(128)S(6)} %select_n.29), kind=kOutput, calls=%fused_computation.2 | convolution fusion | flops 2416508928 | bytes 18350084 | tf_op jit(solution)/shard_map/dot_general | solution.py:705
  230.0 2.1 fusion.22
  237.5 2.2 fusion.135
  239.8 2.5 fusion.43
  242.6 1.8 concatenate.77
  245.1 7.3 %fusion.47 = bf16[3072,64]{0,1:T(8,128)(2,1)S(1)} fusion(f32[3102,64]{0,1:T(8,128)S(1)} %pad_convert_fusion, f32[64]{0:T(128)S(1)} %copy-done.63, f32[64]{0:T(128)S(1)} %copy-done.34, f32[64]{0:T(128)S(1)} %copy-done.35, f32[64]{0:T(128)S(1)} %copy-done.36, f32[64]{0:T(128)S(1)} %copy-done.37, f32[64]{0:T(128)S(1)} %copy-done.38, f32[64]{0:T(128)S(1)} %copy-done.39, ...), kind=kLoop, calls=%fused_computation.54 | loop fusion | flops 12189696 | bytes 24780544 | tf_op jit(solution)/shard_map/convert_element_type | solution.py:716
  254.2 36.5 %shard_map.195 = (bf16[16,192,128]{2,1,0:T(8,128)(2,1)}, f32[16,4,128]{2,1,0:T(4,128)}) custom-call(bf16[16,192,128]{2,1,0:T(8,128)(2,1)} %pad_maximum_fusion.mixed_ref, f32[4,128]{1,0:T(4,128)} %reshape.497.last_ref), custom_call_target="tpu_custom_call" | custom-call | tf_op jit(solution)/shard_map/pallas_call | solution.py:565
  297.1 54.0 %shard_map.196 = bf16[2,768,2048]{2,1,0:T(8,128)(2,1)} custom-call(bf16[2,192,1024]{2,1,0:T(8,128)(2,1)} %pad_maximum_fusion.1.own_ref), custom_call_target="tpu_custom_call" | custom-call | tf_op jit(solution)/shard_map/pallas_call | solution.py:629
  351.1 6.3 %fusion = f32[768,1024]{1,0:T(8,128)S(1)} fusion(bf16[2048,1536]{1,0:T(8,128)(2,1)} %all-gather.2.cloned.1.call-done, bf16[2,768,2048]{2,1,0:T(8,128)(2,1)} %shard_map.196), kind=kOutput, calls=%fused_computation | convolution fusion | flops 3221225472 | bytes 10485760 | tf_op jit(solution)/shard_map/dot_general | solution.py:742
  357.5 4.4 %fusion.15 = bf16[768,512]{1,0:T(8,128)(2,1)} fusion(f32[768,1024]{1,0:T(8,128)S(1)} %fusion, bf16[2048,1536]{1,0:T(8,128)(2,1)} %all-gather.2.cloned.1.call-done, bf16[2,768,2048]{2,1,0:T(8,128)(2,1)S(1)} %copy-done.1), kind=kOutput, calls=%fused_computation.21 | convolution fusion | flops 1612972032 | bytes 9175040 | tf_op jit(solution)/shard_map/dot_general | solution.py:741
  361.9 3.5 all-to-all-start
  366.1 10.9 %all-to-all-done = bf16[4,192,512]{2,1,0:T(8,128)(2,1)S(1)} async-done(((bf16[4,192,512]{2,1,0:T(8,128)(2,1)}), bf16[4,192,512]{2,1,0:T(8,128)(2,1)S(1)}, u32[]{:S(2)}, u32[]{:S(2)}) %all-to-all-start) | async-done | bytes 786464 | tf_op jit(solution)/shard_map/all_to_all | solution.py:747
  (263 shorter events, 41.9 us)
Async XLA Ops:
  7.2 344.0 %all-gather.2.cloned.1.call-start = ((), (), s32[]{:S(2)}) async-start(), calls=%async_computation.1 | async-start | bytes 7864320 | tf_op jit(solution)/shard_map/all_gather | solution.py:687
  18.4 3.7 copy-start.32
  185.8 33.2 %collective-permute-start = (f32[3072,192]{0,1:T(8,128)}, f32[3072,192]{0,1:T(8,128)}, u32[]{:S(2)}, u32[]{:S(2)}) collective-permute-start(f32[3072,192]{0,1:T(8,128)} %fusion.29), channel_id=1, source_target_pairs={{0,1},{1,0},{2,3},{3,2},{4,5},{5,4},{6,7},{7,6},{8,9},{9,8},{10,11... | collective-permute-start | bytes 7077896 | tf_op jit(solution)/shard_map/ppermute | solution.py:704
  188.9 13.3 %copy-start.13 = (f32[256]{0:T(256)}, f32[256]{0:T(256)S(1)}, u32[]{:S(2)}) copy-start(f32[256]{0:T(256)S(1)} %reshape_squeeze.6) | copy-start | bytes 3076
  189.0 13.2 %copy-start.15 = (f32[256]{0:T(256)}, f32[256]{0:T(256)S(1)}, u32[]{:S(2)}) copy-start(f32[256]{0:T(256)S(1)} %reshape_squeeze.7) | copy-start | bytes 3076
  202.1 3.4 copy-start.4
  212.0 6.4 %copy-start.12 = (f32[256]{0:T(256)S(1)}, f32[256]{0:T(256)}, u32[]{:S(2)}) copy-start(f32[256]{0:T(256)} %get-tuple-element.14) | copy-start | bytes 3076
  235.5 4.2 %copy-start.5 = (f32[256,512]{0,1:T(8,128)S(1)}, f32[256,512]{0,1:T(8,128)}, u32[]{:S(2)}) copy-start(f32[256,512]{0,1:T(8,128)} %mul.1975) | copy-start | bytes 1572868
  235.5 4.2 %copy-start.64 = (f32[512]{0:T(512)S(1)}, f32[512]{0:T(512)}, u32[]{:S(2)}) copy-start(f32[512]{0:T(512)} %mul.1979) | copy-start | bytes 6148
  235.5 4.2 %copy-start.65 = (f32[1,256]{1,0:T(1,128)S(1)}, f32[1,256]{1,0:T(1,128)}, u32[]{:S(2)}) copy-start(f32[1,256]{1,0:T(1,128)} %slice.449) | copy-start | bytes 3076
  235.5 4.2 %copy-start.66 = (f32[1,256]{1,0:T(1,128)S(1)}, f32[1,256]{1,0:T(1,128)}, u32[]{:S(2)}) copy-start(f32[1,256]{1,0:T(1,128)} %slice.478) | copy-start | bytes 3076
  242.3 2.5 copy-start.37
  242.4 2.5 copy-start.38
  242.4 2.5 copy-start.39
  242.4 2.5 copy-start.40
  242.4 2.5 copy-start.41
  242.4 2.5 copy-start.42
  242.4 2.5 copy-start.43
  242.4 2.5 copy-start.44
  290.7 3.1 copy-start
  293.7 2.0 collective-permute-start.1
  351.1 6.3 %copy-start.1 = (bf16[2,768,2048]{2,1,0:T(8,128)(2,1)S(1)}, bf16[2,768,2048]{2,1,0:T(8,128)(2,1)}, u32[]{:S(2)}) copy-start(bf16[2,768,2048]{2,1,0:T(8,128)(2,1)} %shard_map.196) | copy-start | bytes 18874372
  357.5 7.9 %copy-start.11 = (f32[16,4,128]{2,1,0:T(4,128)S(1)}, f32[16,4,128]{2,1,0:T(4,128)}, u32[]{:S(2)}) copy-start(f32[16,4,128]{2,1,0:T(4,128)} %get-tuple-element.11) | copy-start | bytes 98308
  361.9 15.1 %all-to-all-start = ((bf16[4,192,512]{2,1,0:T(8,128)(2,1)}), bf16[4,192,512]{2,1,0:T(8,128)(2,1)S(1)}, u32[]{:S(2)}, u32[]{:S(2)}) async-start(bf16[4,192,512]{2,1,0:T(8,128)(2,1)} %bitcast.66), calls=%async_computation | async-start | bytes 1572864 | tf_op jit(solution)/shard_map/all_to_all | solution.py:747
  (49 other events, 84.1 us)
Sparse Core Ops, SparseCore 0:
  187.2 136.5 all-gather.1

commit v2 on v1

--- a/solution.py
+++ b/solution.py
@@ -673,17 +673,17 @@
     own_half = lax.dynamic_slice_in_dim(normed, core * half, half, axis=1)
     rows, wide = conv_value.shape
     share = wide // devices
-    in_block = jnp.stack([conv_value, conv_gate, state_feed], axis=1)
-    in_block = in_block.reshape(rows, 3, devices, share).transpose(2, 0, 1, 3)
-    in_block = in_block.reshape(devices, rows, 3 * share)
+    in_block = jnp.concatenate(
+        [weight.T.reshape(devices, share, rows) for weight in (conv_value, conv_gate, state_feed)],
+        axis=1,
+    )
     out_rows, columns = conv_project.shape
     piece = columns // inner
     all_half, in_block, out_block = entry_exchange(
         own_half, in_block, (conv_project, state_value, state_gate), lax.axis_size("outer")
     )
-    in_block = in_block.reshape(2, half, 3 * share)
-    kept = lax.dynamic_index_in_dim(in_block, core, axis=0, keepdims=False)
-    taken = lax.dynamic_index_in_dim(in_block, 1 - core, axis=0, keepdims=False)
+    in_block = in_block.reshape(2, devices // 2, 3 * share, rows).transpose(0, 2, 1, 3)
+    in_block = in_block.reshape(6 * share, half)
     out_block = lax.all_gather(out_block, "outer", axis=0, tiled=True)
     groups = decay_rate.shape[0] // devices
     chunk = 8
@@ -701,8 +701,12 @@
         total,
         chunk,
     )
-    other = lax.ppermute(jnp.dot(all_half, taken, preferred_element_type=jnp.float32), "tp", swap)
-    projected = jnp.dot(all_half, kept, preferred_element_type=jnp.float32) + other
+    partial = lax.dot_general(
+        in_block, all_half, (((1,), (1,)), ((), ())), preferred_element_type=jnp.float32
+    ).reshape(2, 3 * share, total)
+    other = lax.dynamic_index_in_dim(partial, 1 - core, axis=0, keepdims=False)
+    kept = lax.dynamic_index_in_dim(partial, core, axis=0, keepdims=False)
+    projected = (kept + lax.ppermute(other, "tp", swap)).T
     gated = (projected[:, :share] * jax.nn.sigmoid(projected[:, share : 2 * share])).astype(
         jnp.bfloat16
     )

time: 386 us -> 370 us (0.959)
  matrix products: 43.5 us -> 34.9 us
  Pallas kernels: 243 us -> 236 us
    dot_general x2 -> x1, matrix products: 20.5 us -> 10.2 us  [channel_local(): lax.dot_general(in_block, all_half, (((1,), (1,)), ((), ())), preferred_e...]
    unnamed x147 -> x132, local copies, waits for them, and re-layouts: 10.9 us -> 3.95 us
    pallas_call x1, Pallas kernels: 152 us -> 146 us  [entry_exchange(): pl.pallas_call(functools.partial(entry_kernel, depth), out_shape=(jax.Sha...]
    transpose x1 -> x3, local copies, waits for them, and re-layouts: 1.26 us -> 6.13 us  [channel_local(): weight.T.reshape(devices, share, rows)]
    pallas_call x1, Pallas kernels: 36.5 us -> 32.5 us  [middle_exchange(): pl.pallas_call(functools.partial(middle_kernel, depth), out_shape=(jax.Sh...]
  transfers between devices with their start and end apart: 4 -> 4, of which waited for: 1 -> 1; matrix products, arithmetic and copies ran while one was open for 18% -> 16% of each run, Pallas kernels for 24% -> 24%
where the time goes in v2:
time: 370 us; the launch traced here: 369 us
  Pallas kernels  236 us (64%)
  local copies, waits for them, and re-layouts  37.4 us (10%)
  matrix products  34.9 us (9%)
  other arithmetic  27.8 us (8%)
  between operations  15.5 us (4%)
  waiting for transfers between devices  10.9 us (3%)
  starting transfers between devices  6.81 us (2%)
    pallas_call x1, Pallas kernels, entry_exchange(): pl.pallas_call(functools.partial(entry_kernel, depth), out_shape=(jax.Sha...  146 us
    pallas_call x1, Pallas kernels, exit_gather(): pl.pallas_call(exit_kernel, out_shape=jax.ShapeDtypeStruct((parts, 4 * le...  56.5 us
    pallas_call x1, Pallas kernels, middle_exchange(): pl.pallas_call(functools.partial(middle_kernel, depth), out_shape=(jax.Sh...  32.5 us
    all_to_all x1, waiting for transfers between devices, channel_local(): mixer = lax.all_to_all(mixer, 'inner', 0, 0, tiled=True)  10.9 us
    dot_general x1, matrix products, channel_local(): lax.dot_general(in_block, all_half, (((1,), (1,)), ((), ())), preferred_e...  10.2 us
  transfers between devices with their start and end apart: 4, of which 1 were waited for; matrix products, arithmetic and copies ran while one was open for 16% of the time, Pallas kernels for 24%

profile of v2, /device:TPU:0, one launch (start us, length us, event | category | flops | bytes accessed | tf_op | source)
XLA Modules:
  0.0 368.8 jit_solution(16140230743303860905)
XLA Ops:
  7.2 1.9 convert_element_type.98
  9.5 2.1 copy.34
  11.6 2.0 copy.35
  13.6 2.0 copy.36
  18.5 146.5 %shard_map.194 = (bf16[3072,2048]{1,0:T(8,128)(2,1)}, bf16[16,192,256]{2,1,0:T(8,128)(2,1)}, bf16[512,1536]{1,0:T(8,128)(2,1)}) custom-call(bf16[192,2048]{1,0:T(8,128)(2,1)} %fusion.17.own_ref, bf16[16,192,256]{2,1,0:T(8,128)(2,1)} %pad_maximum_fusion.in_ref, bf16[128,2048]{1,0:T(8,128)(2,1)} %project_ref.1, bf16[128,2048]{1,0:T(8,128)(2,1)} %value_ref.1, ...), custom_call_target="tpu_custom_call" | custom-call | tf_op jit(solution)/shard_map/pallas_call | solution.py:498
  165.0 1.6 copy.55
  166.7 10.2 %fusion = f32[2,192,3072]{2,1,0:T(8,128)} fusion(bf16[2,192,2048]{2,1,0:T(8,128)(2,1)S(1)} %bitcast.171, bf16[3072,2048]{1,0:T(8,128)(2,1)} %get-tuple-element.8), kind=kOutput, calls=%fused_computation | convolution fusion | flops 4831838208 | bytes 18874368 | tf_op jit(solution)/shard_map/dot_general | solution.py:704
  176.9 3.3 dynamic-slice_bitcast_fusion
  180.1 3.2 collective-permute-start
  196.5 2.7 fusion.107
  199.2 2.7 fusion.24
  204.6 1.7 dynamic-slice_bitcast_fusion.30
  206.2 2.0 fusion.128
  210.9 2.6 fusion.9
  214.4 2.1 fusion.25
  221.6 2.3 fusion.131
  224.0 3.8 %fusion.41 = bf16[384,512]{1,0:T(8,128)(2,1)} fusion(f32[384,512]{1,0:T(8,128)S(1)} %fusion.131, f32[256,512]{0,1:T(8,128)} %mul.1978, f32[256,512]{0,1:T(8,128)S(1)} %copy-done.7, f32[383,256]{1,0:T(8,128)} %bitcast.178, f32[1,256]{1,0:T(1,128)S(1)} %copy-done.60, f32[383,256]{1,0:T(8,128)} %bitcast.177, f32[1,256]{1,0:T(1,128)S(1)} %copy-done.59, ...), kind=kOutput, calls=%fused_computation.48 | convolution fusion | flops 1211367424 | bytes 3409920 | tf_op jit(solution)/shard_map/dot_general | solution.py:265
  230.4 7.3 %fusion.45 = bf16[3072,64]{0,1:T(8,128)(2,1)S(1)} fusion(f32[3102,64]{0,1:T(8,128)S(1)} %pad_convert_fusion, f32[64]{0:T(128)S(1)} %copy-done.57, f32[64]{0:T(128)S(1)} %copy-done.28, f32[64]{0:T(128)S(1)} %copy-done.29, f32[64]{0:T(128)S(1)} %copy-done.30, f32[64]{0:T(128)S(1)} %copy-done.31, f32[64]{0:T(128)S(1)} %copy-done.32, f32[64]{0:T(128)S(1)} %copy-done.33, ...), kind=kLoop, calls=%fused_computation.53 | loop fusion | flops 12189696 | bytes 24780544 | tf_op jit(solution)/shard_map/convert_element_type | solution.py:720
  239.4 32.5 %shard_map.195 = (bf16[16,192,128]{2,1,0:T(8,128)(2,1)}, f32[16,4,128]{2,1,0:T(4,128)}) custom-call(bf16[16,192,128]{2,1,0:T(8,128)(2,1)} %pad_maximum_fusion.1.mixed_ref, f32[4,128]{1,0:T(4,128)} %reshape.502.last_ref), custom_call_target="tpu_custom_call" | custom-call | tf_op jit(solution)/shard_map/pallas_call | solution.py:565
  278.3 56.5 %shard_map.196 = bf16[2,768,2048]{2,1,0:T(8,128)(2,1)} custom-call(bf16[2,192,1024]{2,1,0:T(8,128)(2,1)} %pad_maximum_fusion.2.own_ref), custom_call_target="tpu_custom_call" | custom-call | tf_op jit(solution)/shard_map/pallas_call | solution.py:629
  334.9 6.6 %fusion.2 = f32[768,1024]{1,0:T(8,128)S(1)} fusion(bf16[2048,1536]{1,0:T(8,128)(2,1)} %all-gather.2.cloned.1.call-done, bf16[2,768,2048]{2,1,0:T(8,128)(2,1)} %shard_map.196), kind=kOutput, calls=%fused_computation.2 | convolution fusion | flops 3221225472 | bytes 10485760 | tf_op jit(solution)/shard_map/dot_general | solution.py:746
  341.5 4.4 %fusion.18 = bf16[768,512]{1,0:T(8,128)(2,1)} fusion(f32[768,1024]{1,0:T(8,128)S(1)} %fusion.2, bf16[2048,1536]{1,0:T(8,128)(2,1)} %all-gather.2.cloned.1.call-done, bf16[2,768,2048]{2,1,0:T(8,128)(2,1)S(1)} %copy-done.1), kind=kOutput, calls=%fused_computation.25 | convolution fusion | flops 1612972032 | bytes 9175040 | tf_op jit(solution)/shard_map/dot_general | solution.py:745
  345.9 3.5 all-to-all-start
  350.1 10.9 %all-to-all-done = bf16[4,192,512]{2,1,0:T(8,128)(2,1)S(1)} async-done(((bf16[4,192,512]{2,1,0:T(8,128)(2,1)}), bf16[4,192,512]{2,1,0:T(8,128)(2,1)S(1)}, u32[]{:S(2)}, u32[]{:S(2)}) %all-to-all-start) | async-done | bytes 786464 | tf_op jit(solution)/shard_map/all_to_all | solution.py:751
  (251 shorter events, 38.9 us)
Async XLA Ops:
  7.2 327.7 %all-gather.2.cloned.1.call-start = ((), (), s32[]{:S(2)}) async-start(), calls=%async_computation.1 | async-start | bytes 7864320 | tf_op jit(solution)/shard_map/all_gather | solution.py:687
  9.1 6.6 %copy-start.26 = (f32[4096]{0:T(1024)S(1)}, f32[4096]{0:T(1024)}, u32[]{:S(2)}) copy-start(f32[4096]{0:T(1024)} %param.20) | copy-start | bytes 49156
  180.1 30.8 %collective-permute-start = (f32[192,3072]{1,0:T(8,128)}, f32[192,3072]{1,0:T(8,128)}, u32[]{:S(2)}, u32[]{:S(2)}) collective-permute-start(f32[192,3072]{1,0:T(8,128)} %dynamic-slice_bitcast_fusion), channel_id=1, source_target_pairs={{0,1},{1,0},{2,3},{3,2},{4,5},{5,4},{6,7},{7,6},{8,9},{9,8},{10,11... | collective-permute-start | bytes 7077896 | tf_op jit(solution)/shard_map/ppermute | solution.py:709
  219.5 4.5 %copy-start.7 = (f32[256,512]{0,1:T(8,128)S(1)}, f32[256,512]{0,1:T(8,128)}, u32[]{:S(2)}) copy-start(f32[256,512]{0,1:T(8,128)} %mul.1975) | copy-start | bytes 1572868
  219.5 4.5 %copy-start.58 = (f32[512]{0:T(512)S(1)}, f32[512]{0:T(512)}, u32[]{:S(2)}) copy-start(f32[512]{0:T(512)} %mul.1979) | copy-start | bytes 6148
  219.5 4.5 %copy-start.59 = (f32[1,256]{1,0:T(1,128)S(1)}, f32[1,256]{1,0:T(1,128)}, u32[]{:S(2)}) copy-start(f32[1,256]{1,0:T(1,128)} %slice.449) | copy-start | bytes 3076
  219.5 4.5 %copy-start.60 = (f32[1,256]{1,0:T(1,128)S(1)}, f32[1,256]{1,0:T(1,128)}, u32[]{:S(2)}) copy-start(f32[1,256]{1,0:T(1,128)} %slice.478) | copy-start | bytes 3076
  227.8 2.3 copy-start.31
  227.8 2.3 copy-start.32
  227.9 2.3 copy-start.33
  227.9 2.3 copy-start.34
  227.9 2.3 copy-start.35
  227.9 2.3 copy-start.36
  227.9 2.3 copy-start.37
  227.9 2.3 copy-start.38
  227.9 2.3 copy-start.39
  227.9 2.3 copy-start.40
  227.9 2.3 copy-start.41
  227.9 2.3 copy-start.42
  272.0 3.1 copy-start
  275.0 2.0 collective-permute-start.1
  334.9 6.6 %copy-start.1 = (bf16[2,768,2048]{2,1,0:T(8,128)(2,1)S(1)}, bf16[2,768,2048]{2,1,0:T(8,128)(2,1)}, u32[]{:S(2)}) copy-start(bf16[2,768,2048]{2,1,0:T(8,128)(2,1)} %shard_map.196) | copy-start | bytes 18874372
  341.5 7.9 %copy-start.10 = (f32[16,4,128]{2,1,0:T(4,128)S(1)}, f32[16,4,128]{2,1,0:T(4,128)}, u32[]{:S(2)}) copy-start(f32[16,4,128]{2,1,0:T(4,128)} %get-tuple-element.11) | copy-start | bytes 98308
  345.9 15.1 %all-to-all-start = ((bf16[4,192,512]{2,1,0:T(8,128)(2,1)}), bf16[4,192,512]{2,1,0:T(8,128)(2,1)S(1)}, u32[]{:S(2)}, u32[]{:S(2)}) async-start(bf16[4,192,512]{2,1,0:T(8,128)(2,1)} %bitcast.70), calls=%async_computation | async-start | bytes 1572864 | tf_op jit(solution)/shard_map/all_to_all | solution.py:751
  (43 other events, 65.3 us)
Sparse Core Ops, SparseCore 0:
  183.5 132.3 all-gather.1
